TPU v7x, 32 devices: a whole 2x2x4 slice. The times are simulated.
32 devices in a mesh: rep: 2 (over x), fs: 8 (over z, y), tp: 2 (over core).
Axes of the slice: x: 2, y: 2, z: 4, core: 2. Of those that a mesh axis runs over, the one named last changes fastest.
Arguments:
- tokens: bfloat16 [5120, 2048], P(('rep', 'fs')), may hold values from -6 to 6
- gate_weight: float32 [2048, 5120], P('fs', 'tp'), may hold values from -0.125 to 0.125
- up_weight: float32 [2048, 5120], P('fs', 'tp'), may hold values from -0.125 to 0.125
- down_weight: float32 [2048, 5120], P('fs', 'tp'), may hold values from -0.078125 to 0.078125
- value_weight: float32 [2048, 2048], P('fs', 'tp'), may hold values from -0.125 to 0.125
- glu_weight: float32 [2048, 2048], P('fs', 'tp'), may hold values from -0.125 to 0.125
- out_weight: float32 [2048, 2048], P('fs', 'tp'), may hold values from -0.125 to 0.125
- gate_scale: float32 [5120], P('tp'), may hold values from 0.1 to 1.9
- up_scale: float32 [5120], P('tp'), may hold values from 0.5 to 2
- down_scale: float32 [2048], P('fs'), may hold values from 1 to 4
- value_scale: float32 [2048], P('tp'), may hold values from 0.2 to 3.4
- glu_scale: float32 [2048], P('tp'), may hold values from 0.1 to 1.9
- out_scale: float32 [2048], P('fs'), may hold values from 1 to 4
- conv_kernel: float32 [31, 2048], P(None, 'tp'), may hold values from -1 to 1
- norm_gain: float32 [2048], P('tp'), may hold values from 0.1 to 1.9
- first_gain: float32 [2048], replicated, may hold values from 0.1 to 1.9
- conv_gain: float32 [2048], replicated, may hold values from 0.1 to 1.9
- second_gain: float32 [2048], replicated, may hold values from 0.1 to 1.9
Outputs:
- result: bfloat16 [5120, 2048], P(('rep', 'fs'))
All inputs are finite; a program needn't handle non-finite values.
Results may differ from a plain program's by a relative error of at most 0.02.
Values may be sent and summed in bfloat16 or wider, within the bound.
A program may use at most 128 MiB of HBM per device.

v0:
```python
import jax
import jax.numpy as jnp
from jax import lax
from jax.sharding import PartitionSpec as P

D = 2048


EPSILON = 1e-06


def rms_rows(rows, gains):
    values = rows.astype(jnp.float32)
    scaled = values * lax.rsqrt(jnp.mean(values * values, axis=-1, keepdims=True) + EPSILON)
    return (scaled * gains).astype(jnp.bfloat16)


def gated_hidden(normed, gate_full, up_full, gate_scale, up_scale):
    gate_part = jnp.dot(normed, gate_full, preferred_element_type=jnp.float32) * gate_scale
    upward = jnp.dot(normed, up_full, preferred_element_type=jnp.float32) * up_scale
    return (jax.nn.silu(gate_part) * upward).astype(jnp.bfloat16)


def causal_depthwise(inputs, kernel):
    taps = kernel.shape[0]
    length = inputs.shape[0]
    padded = jnp.concatenate(
        [jnp.zeros((taps - 1, inputs.shape[1]), jnp.float32), inputs.astype(jnp.float32)], axis=0
    )
    total = jnp.zeros((length, inputs.shape[1]), jnp.float32)
    for offset in range(taps):
        total = total + kernel[offset] * padded[offset : offset + length]
    return total


def branch_sum(active, weight_rows):
    return lax.psum_scatter(
        lax.dot_general(
            active, weight_rows, (((1,), (1,)), ((), ())), preferred_element_type=jnp.float32
        ).astype(jnp.bfloat16),
        "tp",
        scatter_dimension=0,
        tiled=True,
    ).astype(jnp.float32)


def local(
    tokens,
    gate_weight,
    up_weight,
    down_weight,
    value_weight,
    glu_weight,
    out_weight,
    gate_scale,
    up_scale,
    down_scale,
    value_scale,
    glu_scale,
    out_scale,
    conv_kernel,
    norm_gain,
    first_gain,
    conv_gain,
    second_gain,
):
    gate_cast = gate_weight.astype(jnp.bfloat16)
    up_cast = up_weight.astype(jnp.bfloat16)
    down_cast = down_weight.astype(jnp.bfloat16)
    value_cast = value_weight.astype(jnp.bfloat16)
    glu_cast = glu_weight.astype(jnp.bfloat16)
    out_cast = out_weight.astype(jnp.bfloat16)
    gate_full, up_full, down_full, value_full, glu_full, out_full = (
        lax.all_gather(gate_cast, "fs", axis=0, tiled=True),
        lax.all_gather(up_cast, "fs", axis=0, tiled=True),
        lax.all_gather(down_cast, "fs", axis=0, tiled=True),
        lax.all_gather(value_cast, "fs", axis=0, tiled=True),
        lax.all_gather(glu_cast, "fs", axis=0, tiled=True),
        lax.all_gather(out_cast, "fs", axis=0, tiled=True),
    )
    down_rows, out_rows = (
        lax.all_gather(down_scale, "fs", axis=0, tiled=True),
        lax.all_gather(out_scale, "fs", axis=0, tiled=True),
    )
    members = lax.axis_size("tp")
    own_rows = tokens.shape[0] // members
    first_row = lax.axis_index("tp") * own_rows
    hidden = gated_hidden(rms_rows(tokens, first_gain), gate_full, up_full, gate_scale, up_scale)
    own_tokens = lax.dynamic_slice_in_dim(tokens, first_row, own_rows, 0)
    after_first = (
        own_tokens.astype(jnp.float32) + 0.5 * down_rows * branch_sum(hidden, down_full)
    ).astype(jnp.bfloat16)
    rows = lax.all_gather(rms_rows(after_first, conv_gain), "tp", axis=0, tiled=True)
    value_part = jnp.dot(rows, value_full, preferred_element_type=jnp.float32) * value_scale
    gate_part = jnp.dot(rows, glu_full, preferred_element_type=jnp.float32) * glu_scale
    glu_in = (value_part * jax.nn.sigmoid(gate_part)).astype(jnp.bfloat16)
    mixed = causal_depthwise(glu_in, conv_kernel)
    row_sums, row_squares = lax.psum((jnp.sum(mixed, axis=1), jnp.sum(mixed * mixed, axis=1)), "tp")
    mean_rows = (row_sums / D)[:, None]
    square_rows = (row_squares / D)[:, None]
    normalized = (
        (mixed - mean_rows) * lax.rsqrt(square_rows - mean_rows * mean_rows + EPSILON) * norm_gain
    )
    active = jax.nn.silu(normalized).astype(jnp.bfloat16)
    after_conv = (after_first.astype(jnp.float32) + out_rows * branch_sum(active, out_full)).astype(
        jnp.bfloat16
    )
    hidden = gated_hidden(
        lax.all_gather(rms_rows(after_conv, second_gain), "tp", axis=0, tiled=True),
        gate_full,
        up_full,
        gate_scale,
        up_scale,
    )
    after_second = (
        after_conv.astype(jnp.float32) + 0.5 * down_rows * branch_sum(hidden, down_full)
    ).astype(jnp.bfloat16)
    return lax.all_gather(after_second, "tp", axis=0, tiled=True)


def solution(mesh):
    placed = (
        P(("rep", "fs"), None),
        P("fs", "tp"),
        P("fs", "tp"),
        P("fs", "tp"),
        P("fs", "tp"),
        P("fs", "tp"),
        P("fs", "tp"),
        P("tp"),
        P("tp"),
        P("fs"),
        P("tp"),
        P("tp"),
        P("fs"),
        P(None, "tp"),
        P("tp"),
        P(),
        P(),
        P(),
    )
    return jax.shard_map(
        local, mesh=mesh, in_specs=placed, out_specs=P(("rep", "fs"), None), check_vma=False
    )
```

profile of v0, /device:TPU:0, one launch (start us, length us, event | category | flops | bytes accessed | tf_op | source)
XLA Modules:
  0.0 814.5 jit_solution(17534213961294974461)
XLA Ops:
  6.5 3.1 convert_element_type.86
  9.7 1.2 convert_element_type.87
  11.0 2.9 convert_element_type.89
  14.0 1.2 copy-done
  15.6 147.5 %all-gather.12.cloned.1.call-done = bf16[2048,2560]{1,0:T(8,128)(2,1)} async-done(((bf16[256,2560]{1,0:T(8,128)(2,1)}), bf16[2048,2560]{1,0:T(8,128)(2,1)}) %all-gather.12.cloned.1.call-update) | async-done | bytes 10485776 | tf_op jit(solution)/shard_map/all_gather | solution.py:74
  163.1 9.3 %convolution_multiply_fusion.3 = f32[320,2560]{1,0:T(8,128)} fusion(bf16[2048,2560]{1,0:T(8,128)(2,1)} %all-gather.12.cloned.1.call-done, f32[2560]{0:T(1024)S(1)} %copy-done.12, bf16[320,2048]{1,0:T(8,128)(2,1)S(1)} %copy-done, f32[2048]{0:T(1024)S(1)} %copy-done.14, f32[320]{0:T(512)S(1)} %add_rsqrt_fusion.1), kind=kOutput, calls=%fused_computation.5 | convolution fusion | flops 3358883840 | bytes 15092992 | tf_op jit(solution)/shard_map/dot_general | solution.py:19
  172.3 141.6 %all-gather.14.cloned.1.call-done = bf16[2048,2560]{1,0:T(8,128)(2,1)} async-done(((bf16[256,2560]{1,0:T(8,128)(2,1)}), bf16[2048,2560]{1,0:T(8,128)(2,1)}) %all-gather.14.cloned.1.call-update) | async-done | bytes 10485776 | tf_op jit(solution)/shard_map/all_gather | solution.py:75
  314.0 150.9 %all-gather.16.cloned.1.call-done = bf16[2048,2560]{1,0:T(8,128)(2,1)} async-done(((bf16[256,2560]{1,0:T(8,128)(2,1)}), bf16[2048,2560]{1,0:T(8,128)(2,1)}) %all-gather.16.cloned.1.call-update) | async-done | bytes 10485776 | tf_op jit(solution)/shard_map/all_gather | solution.py:76
  464.9 16.1 %convolution_convert_fusion.1 = bf16[320,2048]{1,0:T(8,128)(2,1)} fusion(bf16[2048,2560]{1,0:T(8,128)(2,1)} %all-gather.16.cloned.1.call-done, bf16[2048,2560]{1,0:T(8,128)(2,1)} %all-gather.14.cloned.1.call-done, f32[320,2560]{1,0:T(8,128)} %convolution_multiply_fusion.3, f32[2560]{0:T(1024)S(1)} %copy-done.13, bf16[320,2048]{1,0:T(8,128)(2,1)S(1)} %copy-done, ...), kind=kOutput, calls=%fused_computation.11 | convolution fusion | flops 6719897600 | bytes 26889472 | tf_op jit(solution)/shard_map/dot_general | solution.py:38
  481.1 1.1 copy-done.2
  483.2 17.7 %all-gather = f32[8,1,256]{2,1,0:T(1,128)S(1)} all-gather(f32[1,1,256]{2,1,0:T(1,128)S(1)} %bitcast.96), channel_id=1, replica_groups=mesh['rep'=2,'fs'=8,'tp'=2] {'fs'}, dimensions={0}, use_global_device_ids=true | all-gather | bytes 9216 | tf_op jit(solution)/shard_map/all_gather | solution.py:82
  500.9 1.5 fusion.14
  502.4 1.1 fusion.16
  506.0 58.1 %all-gather.22.cloned.1.call-done = bf16[2048,1024]{1,0:T(8,128)(2,1)} async-done(((bf16[256,1024]{1,0:T(8,128)(2,1)}), bf16[2048,1024]{1,0:T(8,128)(2,1)}) %all-gather.22.cloned.1.call-update) | async-done | bytes 4194320 | tf_op jit(solution)/shard_map/all_gather | solution.py:78
  564.1 9.4 %all-gather.18.cloned.1.call-done = bf16[320,2048]{1,0:T(8,128)(2,1)} async-done(((bf16[160,2048]{1,0:T(8,128)(2,1)}), bf16[320,2048]{1,0:T(8,128)(2,1)}) %all-gather.18.cloned.1.call-update) | async-done | bytes 1310736 | tf_op jit(solution)/shard_map/all_gather | solution.py:93
  573.5 5.4 fusion.11
  578.9 70.7 %all-gather.20.cloned.1.call-done = bf16[2048,1024]{1,0:T(8,128)(2,1)} async-done(((bf16[256,1024]{1,0:T(8,128)(2,1)}), bf16[2048,1024]{1,0:T(8,128)(2,1)}) %all-gather.20.cloned.1.call-update) | async-done | bytes 4194320 | tf_op jit(solution)/shard_map/all_gather | solution.py:77
  649.6 4.1 fusion.13
  653.8 6.3 fusion.84
  660.1 2.5 all-reduce.1
  662.6 60.5 %all-gather.24.cloned.1.call-done = bf16[2048,1024]{1,0:T(8,128)(2,1)} async-done(((bf16[256,1024]{1,0:T(8,128)(2,1)}), bf16[2048,1024]{1,0:T(8,128)(2,1)}) %all-gather.24.cloned.1.call-update) | async-done | bytes 4194320 | tf_op jit(solution)/shard_map/all_gather | solution.py:79
  723.1 5.1 convolution_convert_fusion.2
  728.8 18.1 %all-gather.1 = f32[8,1,256]{2,1,0:T(1,128)S(1)} all-gather(f32[1,1,256]{2,1,0:T(1,128)S(1)} %bitcast.97), channel_id=1, replica_groups=mesh['rep'=2,'fs'=8,'tp'=2] {'fs'}, dimensions={0}, use_global_device_ids=true | all-gather | bytes 9216 | tf_op jit(solution)/shard_map/all_gather | solution.py:83
  747.0 1.5 fusion.18
  748.4 1.1 fusion.20
  749.8 6.5 all-gather.26.cloned.1.call-done
  756.3 9.7 %convolution_multiply_fusion.1 = f32[320,2560]{1,0:T(8,128)} fusion(bf16[320,2048]{1,0:T(8,128)(2,1)} %all-gather.26.cloned.1.call-done, bf16[2048,2560]{1,0:T(8,128)(2,1)} %all-gather.12.cloned.1.call-done, f32[2560]{0:T(1024)S(1)} %copy-done.12), kind=kOutput, calls=%fused_computation.2 | convolution fusion | flops 3356262400 | bytes 15083520 | tf_op jit(solution)/shard_map/dot_general | solution.py:19
  766.0 16.0 %convolution_convert_fusion = bf16[320,2048]{1,0:T(8,128)(2,1)} fusion(bf16[2048,2560]{1,0:T(8,128)(2,1)} %all-gather.16.cloned.1.call-done, bf16[320,2048]{1,0:T(8,128)(2,1)S(1)} %copy-done.11, bf16[2048,2560]{1,0:T(8,128)(2,1)} %all-gather.14.cloned.1.call-done, f32[320,2560]{1,0:T(8,128)} %convolution_multiply_fusion.1, f32[2560]{0:T(1024)S(1)} %copy-done.13), kind=kOutput, calls=%fused_computation.10 | convolution fusion | flops 6717276160 | bytes 26880000 | tf_op jit(solution)/shard_map/dot_general | solution.py:38
  782.1 10.0 %reduce-scatter.8.cloned.1.call-done = bf16[160,2048]{1,0:T(8,128)(2,1)} async-done(((bf16[320,2048]{1,0:T(8,128)(2,1)}), bf16[160,2048]{1,0:T(8,128)(2,1)}) %reduce-scatter.8.cloned.1.call-update) | async-done | bytes 655376 | tf_op jit(solution)/shard_map/reduce_scatter | solution.py:37
  792.1 2.2 fusion.21
  794.3 10.9 %all-gather.28.cloned.1.call-done = bf16[320,2048]{1,0:T(8,128)(2,1)} async-done(((bf16[160,2048]{1,0:T(8,128)(2,1)}), bf16[320,2048]{1,0:T(8,128)(2,1)}) %all-gather.28.cloned.1.call-update) | async-done | bytes 1310736 | tf_op jit(solution)/shard_map/all_gather | solution.py:118
  805.1 2.5 copy.20
  (71 shorter events, 5.1 us)
Async XLA Ops:
  6.5 156.5 %all-gather.12.cloned.1.call-start = ((), (), s32[]{:S(2)}) async-start(), calls=%async_computation.3 | async-start | bytes 11796480 | tf_op jit(solution)/shard_map/all_gather | solution.py:74
  6.5 3.2 copy-start.1
  9.7 304.3 %all-gather.14.cloned.1.call-start = ((), (), s32[]{:S(2)}) async-start(), calls=%async_computation.4 | async-start | bytes 11796480 | tf_op jit(solution)/shard_map/all_gather | solution.py:75
  10.9 454.0 %all-gather.16.cloned.1.call-start = ((), (), s32[]{:S(2)}) async-start(), calls=%async_computation.5 | async-start | bytes 11796480 | tf_op jit(solution)/shard_map/all_gather | solution.py:76
  13.9 1.3 copy-start
  13.9 149.1 %copy-start.12 = (f32[2560]{0:T(1024)S(1)}, f32[2560]{0:T(1024)}, u32[]{:S(2)}) copy-start(f32[2560]{0:T(1024)} %param.25) | copy-start | bytes 30724
  13.9 149.2 %copy-start.14 = (f32[2048]{0:T(1024)S(1)}, f32[2048]{0:T(1024)}, u32[]{:S(2)}) copy-start(f32[2048]{0:T(1024)} %param.33) | copy-start | bytes 24580
  13.9 486.9 %reduce-scatter.4.cloned.1.call-start = ((), (), s32[]{:S(2)}) async-start(), calls=%async_computation.6 | async-start | bytes 1966080 | tf_op jit(solution)/shard_map/reduce_scatter | solution.py:37
  15.6 449.3 %copy-start.13 = (f32[2560]{0:T(1024)S(1)}, f32[2560]{0:T(1024)}, u32[]{:S(2)}) copy-start(f32[2560]{0:T(1024)} %param.26) | copy-start | bytes 30724
  481.0 1.2 copy-start.2
  481.0 2.2 copy-start.8
  481.0 83.1 %all-gather.22.cloned.1.call-start = ((), (), s32[]{:S(2)}) async-start(), calls=%async_computation.9 | async-start | bytes 4718592 | tf_op jit(solution)/shard_map/all_gather | solution.py:78
  483.1 19.3 %copy-start.6 = (f32[2048]{0:T(1024)S(1)}, f32[2048]{0:T(1024)}, u32[]{:S(2)}) copy-start(f32[2048]{0:T(1024)} %param.34) | copy-start | bytes 24580
  483.1 90.4 %all-gather.18.cloned.1.call-start = ((), (), s32[]{:S(2)}) async-start(), calls=%async_computation.7 | async-start | bytes 1966080 | tf_op jit(solution)/shard_map/all_gather | solution.py:93
  502.3 1.4 copy-start.3
  503.4 1.3 copy-start.4
  503.4 146.2 %all-gather.20.cloned.1.call-start = ((), (), s32[]{:S(2)}) async-start(), calls=%async_computation.8 | async-start | bytes 4718592 | tf_op jit(solution)/shard_map/all_gather | solution.py:77
  504.6 1.3 copy-start.5
  504.6 68.9 %copy-start.15 = (f32[1024]{0:T(1024)S(1)}, f32[1024]{0:T(1024)}, u32[]{:S(2)}) copy-start(f32[1024]{0:T(1024)} %param.29) | copy-start | bytes 12292
  504.6 218.5 %all-gather.24.cloned.1.call-start = ((), (), s32[]{:S(2)}) async-start(), calls=%async_computation.10 | async-start | bytes 4718592 | tf_op jit(solution)/shard_map/all_gather | solution.py:79
  505.6 241.4 %reduce-scatter.6.cloned.1.call-start = ((), (), s32[]{:S(2)}) async-start(), calls=%async_computation.11 | async-start | bytes 1966080 | tf_op jit(solution)/shard_map/reduce_scatter | solution.py:37
  506.0 143.7 %copy-start.16 = (f32[1024]{0:T(1024)S(1)}, f32[1024]{0:T(1024)}, u32[]{:S(2)}) copy-start(f32[1024]{0:T(1024)} %param.28) | copy-start | bytes 12292
  573.5 76.1 %copy-start.10 = (bf16[320,2048]{1,0:T(8,128)(2,1)S(1)}, bf16[320,2048]{1,0:T(8,128)(2,1)}, u32[]{:S(2)}) copy-start(bf16[320,2048]{1,0:T(8,128)(2,1)} %all-gather.18.cloned.1.call-done) | copy-start | bytes 3932164
  653.8 69.3 %copy-start.17 = (f32[1024]{0:T(1024)S(1)}, f32[1024]{0:T(1024)}, u32[]{:S(2)}) copy-start(f32[1024]{0:T(1024)} %param.32) | copy-start | bytes 12292
  728.2 0.7 copy-start.9
  728.2 20.2 %copy-start.7 = (f32[2048]{0:T(1024)S(1)}, f32[2048]{0:T(1024)}, u32[]{:S(2)}) copy-start(f32[2048]{0:T(1024)} %param.35) | copy-start | bytes 24580
  728.2 28.1 %all-gather.26.cloned.1.call-start = ((), (), s32[]{:S(2)}) async-start(), calls=%async_computation.12 | async-start | bytes 1966080 | tf_op jit(solution)/shard_map/all_gather | solution.py:109
  749.5 42.6 %reduce-scatter.8.cloned.1.call-start = ((), (), s32[]{:S(2)}) async-start(), calls=%async_computation.13 | async-start | bytes 1966080 | tf_op jit(solution)/shard_map/reduce_scatter | solution.py:37
  756.3 9.7 %copy-start.11 = (bf16[320,2048]{1,0:T(8,128)(2,1)S(1)}, bf16[320,2048]{1,0:T(8,128)(2,1)}, u32[]{:S(2)}) copy-start(bf16[320,2048]{1,0:T(8,128)(2,1)} %all-gather.26.cloned.1.call-done) | copy-start | bytes 3932164
  782.1 23.1 %all-gather.28.cloned.1.call-start = ((), (), s32[]{:S(2)}) async-start(), calls=%async_computation.14 | async-start | bytes 1966080 | tf_op jit(solution)/shard_map/all_gather | solution.py:118
Sparse Core Ops, SparseCore 0:
  9.8 153.2 all-gather.11
  165.2 148.6 all-gather.13
  316.2 148.6 all-gather.15
  481.1 6.8 reduce-scatter.3
  490.0 74.0 all-gather.21
  565.5 7.9 all-gather.17
  575.6 73.9 all-gather.19
  651.7 71.3 all-gather.23
  728.3 7.2 reduce-scatter.5
  749.6 6.6 all-gather.25
  782.2 9.8 reduce-scatter.7
  794.4 10.6 all-gather.27
where the time goes:
time: 815 us
  waiting for transfers between devices  666 us (82%)
  matrix products  65.7 us (8%)
  blocking collectives  38.2 us (5%)
  other arithmetic  23.8 us (3%)
  between operations  13.7 us (2%)
    all_gather x1, waiting for transfers between devices, local(): lax.all_gather(down_cast, 'fs', axis=0, tiled=True)  151 us
    all_gather x1, waiting for transfers between devices, local(): lax.all_gather(gate_cast, 'fs', axis=0, tiled=True)  147 us
    all_gather x1, waiting for transfers between devices, local(): lax.all_gather(up_cast, 'fs', axis=0, tiled=True)  142 us
    all_gather x1, waiting for transfers between devices, local(): lax.all_gather(value_cast, 'fs', axis=0, tiled=True)  70.7 us
    all_gather x1, waiting for transfers between devices, local(): lax.all_gather(out_cast, 'fs', axis=0, tiled=True)  60.5 us
    all_gather x1, waiting for transfers between devices, local(): lax.all_gather(glu_cast, 'fs', axis=0, tiled=True)  58.1 us
    dot_general x3, matrix products, branch_sum(): lax.dot_general(active, weight_rows, (((1,), (1,)), ((), ())), preferred_...  37.2 us
    dot_general x2, matrix products, gated_hidden(): jnp.dot(normed, gate_full, preferred_element_type=jnp.float32) * gate_scale  19 us
  transfers between devices with their start and end apart: 12, of which 10 were waited for; matrix products, arithmetic and copies ran while one was open for 4% of the time, Pallas kernels for 0%

commit v1 on v0

v1 whole, which is shorter than its diff:
```python
import jax
import jax.numpy as jnp
from jax import lax
from jax.sharding import PartitionSpec as P

D = 2048


EPSILON = 1e-06


def rms_rows(rows, gains):
    values = rows.astype(jnp.float32)
    scaled = values * lax.rsqrt(jnp.mean(values * values, axis=-1, keepdims=True) + EPSILON)
    return (scaled * gains).astype(jnp.bfloat16)


def gated_hidden(normed, gate_full, up_full, gate_scale, up_scale):
    gate_part = jnp.dot(normed, gate_full, preferred_element_type=jnp.float32) * gate_scale
    upward = jnp.dot(normed, up_full, preferred_element_type=jnp.float32) * up_scale
    return (jax.nn.silu(gate_part) * upward).astype(jnp.bfloat16)


def causal_depthwise(inputs, kernel):
    taps = kernel.shape[0]
    length = inputs.shape[0]
    padded = jnp.concatenate(
        [jnp.zeros((taps - 1, inputs.shape[1]), jnp.float32), inputs.astype(jnp.float32)], axis=0
    )
    total = jnp.zeros((length, inputs.shape[1]), jnp.float32)
    for offset in range(taps):
        total = total + kernel[offset] * padded[offset : offset + length]
    return total


def swap(values, axis):
    return lax.ppermute(values, axis, [(0, 1), (1, 0)])


def gather_rows(rows, axis):
    if lax.axis_size(axis) != 2:
        return lax.all_gather(rows, axis, axis=0, tiled=True)
    other = swap(rows, axis)
    first = lax.axis_index(axis) == 0
    return jnp.concatenate([jnp.where(first, rows, other), jnp.where(first, other, rows)], axis=0)


def scatter_rows(partial, axis):
    members = lax.axis_size(axis)
    if members != 2:
        return lax.psum_scatter(partial, axis, scatter_dimension=0, tiled=True).astype(jnp.float32)
    own_rows = partial.shape[0] // members
    place = lax.axis_index(axis)
    mine = lax.dynamic_slice_in_dim(partial, place * own_rows, own_rows, 0)
    theirs = lax.dynamic_slice_in_dim(partial, (1 - place) * own_rows, own_rows, 0)
    return mine.astype(jnp.float32) + swap(theirs, axis).astype(jnp.float32)


def pull(rows, step):
    n = lax.axis_size("rep")
    return lax.ppermute(rows, "rep", [(s, (s - step) % n) for s in range(n)])


def push(rows, step):
    n = lax.axis_size("rep")
    return lax.ppermute(rows, "rep", [(s, (s + step) % n) for s in range(n)])


def streams_of(own):
    n = lax.axis_size("rep")
    parts = [own] + [pull(own, step) for step in range(1, n)]
    return [gather_rows(part, "tp") for part in parts]


def owned_sum(actives, weight_rows):
    n = lax.axis_size("rep")
    total = None
    for step in list(range(1, n)) + [0]:
        partial = lax.dot_general(
            actives[step], weight_rows, (((1,), (1,)), ((), ())), preferred_element_type=jnp.float32
        ).astype(jnp.bfloat16)
        part = scatter_rows(partial, "tp")
        if step:
            part = push(part.astype(jnp.bfloat16), step).astype(jnp.float32)
        total = part if total is None else total + part
    return total


def local(
    tokens,
    gate_weight,
    up_weight,
    down_weight,
    value_weight,
    glu_weight,
    out_weight,
    gate_scale,
    up_scale,
    down_scale,
    value_scale,
    glu_scale,
    out_scale,
    conv_kernel,
    norm_gain,
    first_gain,
    conv_gain,
    second_gain,
):
    reps = lax.axis_size("rep")
    rep = lax.axis_index("rep")

    def part(array, dim):
        width = array.shape[dim] // reps
        return lax.dynamic_slice_in_dim(array, rep * width, width, dim)

    scales = lax.all_gather(jnp.stack([down_scale, out_scale]), "fs", axis=1, tiled=True)
    down_rows, out_rows = scales[0], scales[1]

    def full(weight):
        return lax.all_gather(part(weight, 1).astype(jnp.bfloat16), "fs", axis=0, tiled=True)

    gate_full, up_full, down_full, value_full, glu_full, out_full = (
        full(gate_weight),
        full(up_weight),
        full(down_weight),
        full(value_weight),
        full(glu_weight),
        full(out_weight),
    )
    gate_scale, up_scale, value_scale, glu_scale, norm_gain = (
        part(gate_scale, 0),
        part(up_scale, 0),
        part(value_scale, 0),
        part(glu_scale, 0),
        part(norm_gain, 0),
    )
    conv_kernel = part(conv_kernel, 1)
    members = lax.axis_size("tp")
    own_rows = tokens.shape[0] // members
    own_tokens = lax.dynamic_slice_in_dim(tokens, lax.axis_index("tp") * own_rows, own_rows, 0)

    normed = rms_rows(tokens, first_gain)
    own_normed = rms_rows(own_tokens, first_gain)
    rows = [normed] + [gather_rows(pull(own_normed, step), "tp") for step in range(1, reps)]
    hidden = [gated_hidden(r, gate_full, up_full, gate_scale, up_scale) for r in rows]
    after_first = (
        own_tokens.astype(jnp.float32) + 0.5 * down_rows * owned_sum(hidden, down_full)
    ).astype(jnp.bfloat16)
    mixes, sums = [], []
    for rows in streams_of(rms_rows(after_first, conv_gain)):
        value_part = jnp.dot(rows, value_full, preferred_element_type=jnp.float32) * value_scale
        gate_part = jnp.dot(rows, glu_full, preferred_element_type=jnp.float32) * glu_scale
        glu_in = (value_part * jax.nn.sigmoid(gate_part)).astype(jnp.bfloat16)
        mixed = causal_depthwise(glu_in, conv_kernel)
        mixes.append(mixed)
        sums.append(jnp.stack([jnp.sum(mixed, axis=1), jnp.sum(mixed * mixed, axis=1)]))
    totals = lax.psum(jnp.roll(jnp.stack(sums), rep, axis=0), ("rep", "tp"))
    totals = jnp.roll(totals, -rep, axis=0) / D
    actives = []
    for step, mixed in enumerate(mixes):
        mean_rows = totals[step, 0][:, None]
        square_rows = totals[step, 1][:, None]
        normalized = (
            (mixed - mean_rows) * lax.rsqrt(square_rows - mean_rows * mean_rows + EPSILON) * norm_gain
        )
        actives.append(jax.nn.silu(normalized).astype(jnp.bfloat16))
    after_conv = (after_first.astype(jnp.float32) + out_rows * owned_sum(actives, out_full)).astype(
        jnp.bfloat16
    )
    hidden = [
        gated_hidden(r, gate_full, up_full, gate_scale, up_scale)
        for r in streams_of(rms_rows(after_conv, second_gain))
    ]
    after_second = (
        after_conv.astype(jnp.float32) + 0.5 * down_rows * owned_sum(hidden, down_full)
    ).astype(jnp.bfloat16)
    return gather_rows(after_second, "tp")


def solution(mesh):
    placed = (
        P(("rep", "fs"), None),
        P("fs", "tp"),
        P("fs", "tp"),
        P("fs", "tp"),
        P("fs", "tp"),
        P("fs", "tp"),
        P("fs", "tp"),
        P("tp"),
        P("tp"),
        P("fs"),
        P("tp"),
        P("tp"),
        P("fs"),
        P(None, "tp"),
        P("tp"),
        P(),
        P(),
        P(),
    )
    return jax.shard_map(
        local, mesh=mesh, in_specs=placed, out_specs=P(("rep", "fs"), None), check_vma=False
    )
```

time: 815 us -> 516 us (0.63)
  waiting for transfers between devices: 666 us -> 354 us
  local copies, waits for them, and re-layouts: 5.91 us -> 22.6 us
  starting transfers between devices: 0.86 us -> 11.7 us
  other arithmetic: 23.8 us -> 14.1 us
    all_gather x9 -> x6, waiting for transfers between devices: 656 us -> 283 us  [full(): lax.all_gather(part(weight, 1).astype(jnp.bfloat16), 'fs', axis=0, tiled=...]
    ppermute x0 -> x18, waiting for transfers between devices: none -> 70.8 us  [the longest x3 37.2 us: pull(): return lax.ppermute(rows, 'rep', [(s, (s - step) % n) for s in range(n)])]
    ppermute x0 -> x18, starting transfers between devices: none -> 11.5 us  [the longest x3 5.19 us: pull(): return lax.ppermute(rows, 'rep', [(s, (s - step) % n) for s in range(n)])]
    convert_element_type x7 -> x4, other arithmetic: 12 us -> 1.06 us  [the longest x3 0.61 us: owned_sum(): part = push(part.astype(jnp.bfloat16), step).astype(jnp.float32)]
    convert_element_type x0 -> x6, local copies, waits for them, and re-layouts: none -> 10.8 us  [full(): part(weight, 1).astype(jnp.bfloat16)]
    reduce_scatter x3 -> x0, waiting for transfers between devices: 9.99 us -> none  [branch_sum(): lax.psum_scatter(lax.dot_general(active, weight_rows, (((1,), (1,)), ((),...]
    all_gather x2 -> x1, blocking collectives: 35.8 us -> 26.7 us  [local(): lax.all_gather(jnp.stack([down_scale, out_scale]), 'fs', axis=1, tiled=True)]
    dot_general x3 -> x6, matrix products: 37.2 us -> 39.9 us  [owned_sum(): lax.dot_general(actives[step], weight_rows, (((1,), (1,)), ((), ())), pre...]
  transfers between devices with their start and end apart: 12 -> 24, of which waited for: 10 -> 13; matrix products, arithmetic and copies ran while one was open for 4% -> 15% of each run, Pallas kernels for 0% -> 0%
where the time goes in v1:
time: 516 us; the launch traced here: 515 us
  waiting for transfers between devices  354 us (69%)
  matrix products  65.4 us (13%)
  blocking collectives  33.1 us (6%)
  local copies, waits for them, and re-layouts  22.6 us (4%)
  other arithmetic  14.1 us (3%)
  between operations  14.1 us (3%)
  starting transfers between devices  11.7 us (2%)
    all_gather x6, waiting for transfers between devices, full(): lax.all_gather(part(weight, 1).astype(jnp.bfloat16), 'fs', axis=0, tiled=...  283 us
    dot_general x6, matrix products, owned_sum(): lax.dot_general(actives[step], weight_rows, (((1,), (1,)), ((), ())), pre...  39.9 us
    ppermute x3, waiting for transfers between devices, pull(): return lax.ppermute(rows, 'rep', [(s, (s - step) % n) for s in range(n)])  37.2 us
    ppermute x3, waiting for transfers between devices, push(): return lax.ppermute(rows, 'rep', [(s, (s + step) % n) for s in range(n)])  30.6 us
    all_gather x1, blocking collectives, local(): lax.all_gather(jnp.stack([down_scale, out_scale]), 'fs', axis=1, tiled=True)  26.7 us
    dot_general x4, matrix products, gated_hidden(): jnp.dot(normed, gate_full, preferred_element_type=jnp.float32) * gate_scale  17.5 us
    convert_element_type x6, local copies, waits for them, and re-layouts, full(): part(weight, 1).astype(jnp.bfloat16)  10.8 us
  transfers between devices with their start and end apart: 24, of which 13 were waited for; matrix products, arithmetic and copies ran while one was open for 15% of the time, Pallas kernels for 0%

profile of v1, /device:TPU:0, one launch (start us, length us, event | category | flops | bytes accessed | tf_op | source)
XLA Modules:
  0.0 515.1 jit_solution(11567098746282541957)
XLA Ops:
  9.3 2.2 dynamic-slice_convert_fusion
  11.6 2.4 dynamic-slice_convert_fusion.1
  14.0 1.8 dynamic-slice_convert_fusion.4
  16.4 3.0 collective-permute-start
  19.4 14.7 %collective-permute-done = bf16[160,2048]{1,0:T(8,128)(2,1)S(1)} collective-permute-done((bf16[160,2048]{1,0:T(8,128)(2,1)S(1)}, bf16[160,2048]{1,0:T(8,128)(2,1)S(1)}, u32[]{:S(2)}, u32[]{:S(2)}) %collective-permute-start) | collective-permute-done | bytes 655392 | tf_op jit(solution)/shard_map/ppermute | solution.py:61
  34.1 1.8 dynamic-slice_convert_fusion.5
  37.5 60.7 %all-gather.7.cloned.1.call-done = bf16[2048,1280]{1,0:T(8,128)(2,1)} async-done(((bf16[256,1280]{1,0:T(8,128)(2,1)}), bf16[2048,1280]{1,0:T(8,128)(2,1)}) %all-gather.7.cloned.1.call-update) | async-done | bytes 5242896 | tf_op jit(solution)/shard_map/all_gather | solution.py:120
  98.2 5.8 %convolution_multiply_fusion.7 = f32[320,1280]{1,0:T(8,128)} fusion(bf16[2048,1280]{1,0:T(8,128)(2,1)} %all-gather.7.cloned.1.call-done, bf16[160,2048]{1,0:T(8,128)(2,1)} %get-tuple-element.31, bf16[160,2048]{1,0:T(8,128)(2,1)S(1)} %get-tuple-element.30, f32[1280]{0:T(1024)S(1)} %dynamic_slice.80), kind=kOutput, calls=%fused_computation.13 | convolution fusion | flops 1680752640 | bytes 8197120 | tf_op jit(solution)/shard_map/dot_general | solution.py:19
  103.9 80.5 %all-gather.11.cloned.1.call-done = bf16[2048,1280]{1,0:T(8,128)(2,1)} async-done(((bf16[256,1280]{1,0:T(8,128)(2,1)}), bf16[2048,1280]{1,0:T(8,128)(2,1)}) %all-gather.11.cloned.1.call-update) | async-done | bytes 5242896 | tf_op jit(solution)/shard_map/all_gather | solution.py:120
  184.4 86.3 %all-gather.9.cloned.1.call-done = bf16[2048,1280]{1,0:T(8,128)(2,1)} async-done(((bf16[256,1280]{1,0:T(8,128)(2,1)}), bf16[2048,1280]{1,0:T(8,128)(2,1)}) %all-gather.9.cloned.1.call-update) | async-done | bytes 5242896 | tf_op jit(solution)/shard_map/all_gather | solution.py:120
  270.7 8.8 %convolution_convert_fusion.3 = bf16[320,2048]{1,0:T(8,128)(2,1)S(1)} fusion(bf16[2048,1280]{1,0:T(8,128)(2,1)} %all-gather.11.cloned.1.call-done, bf16[2048,1280]{1,0:T(8,128)(2,1)} %all-gather.9.cloned.1.call-done, f32[320,1280]{1,0:T(8,128)} %convolution_multiply_fusion.7, bf16[160,2048]{1,0:T(8,128)(2,1)S(1)} %copy-done.9, ...), kind=kOutput, calls=%fused_computation.21 | convolution fusion | flops 3361587200 | bytes 14750720 | tf_op jit(solution)/shard_map/dot_general | solution.py:79
  280.8 5.6 %convolution_multiply_fusion.5 = f32[320,1280]{1,0:T(8,128)} fusion(bf16[2048,1280]{1,0:T(8,128)(2,1)} %all-gather.7.cloned.1.call-done, f32[1280]{0:T(1024)S(1)} %dynamic_slice.80, bf16[320,2048]{1,0:T(8,128)(2,1)S(1)} %copy-done.2, f32[2048]{0:T(1024)S(1)} %copy-done.13, f32[320]{0:T(512)S(1)} %add_rsqrt_fusion.2), kind=kOutput, calls=%fused_computation.10 | convolution fusion | flops 1680752640 | bytes 8206592 | tf_op jit(solution)/shard_map/dot_general | solution.py:19
  286.4 8.7 %convolution_convert_fusion.2 = bf16[320,2048]{1,0:T(8,128)(2,1)S(1)} fusion(bf16[2048,1280]{1,0:T(8,128)(2,1)} %all-gather.11.cloned.1.call-done, bf16[2048,1280]{1,0:T(8,128)(2,1)} %all-gather.9.cloned.1.call-done, f32[320,1280]{1,0:T(8,128)} %convolution_multiply_fusion.5, f32[1280]{0:T(1024)S(1)} %dynamic_slice.82, bf16[320,2048]{1,0:T(8,128)(2,1)S(1)} %copy-done.2, ...), kind=kOutput, calls=%fused_computation.20 | convolution fusion | flops 3361587200 | bytes 14760192 | tf_op jit(solution)/shard_map/dot_general | solution.py:79
  298.2 26.7 %all_gather.21 = f32[2,2048]{1,0:T(2,128)S(1)} all-gather(f32[2,256]{1,0:T(2,128)S(1)} %pad_maximum_fusion.22), channel_id=1, replica_groups=mesh['rep'=2,'fs'=8,'tp'=2] {'fs'}, dimensions={1}, use_global_device_ids=true | all-gather | bytes 18432 | tf_op jit(solution)/shard_map/all_gather | solution.py:116
  326.5 1.8 dynamic-slice_convert_fusion.3
  331.2 8.0 %collective-permute-done.5 = bf16[160,2048]{1,0:T(8,128)(2,1)S(1)} collective-permute-done((bf16[160,2048]{1,0:T(8,128)(2,1)S(1)}, bf16[160,2048]{1,0:T(8,128)(2,1)S(1)}, u32[]{:S(2)}, u32[]{:S(2)}) %collective-permute-start.5) | collective-permute-done | bytes 655392 | tf_op jit(solution)/shard_map/ppermute | solution.py:61
  340.5 3.7 fusion.26
  344.1 25.9 %all-gather.13.cloned.1.call-done = bf16[2048,512]{1,0:T(8,128)(2,1)} async-done(((bf16[256,512]{1,0:T(8,128)(2,1)}), bf16[2048,512]{1,0:T(8,128)(2,1)}) %all-gather.13.cloned.1.call-update) | async-done | bytes 2097168 | tf_op jit(solution)/shard_map/all_gather | solution.py:120
  370.0 2.6 fusion.36
  372.6 3.2 fusion.189
  379.9 3.2 fusion.188
  383.2 6.4 %psum.7 = f32[2,2,320]{2,1,0:T(2,128)S(1)} all-reduce(f32[2,2,320]{2,1,0:T(2,128)S(1)} %fusion.167), channel_id=1, replica_groups=mesh['rep'=2,'fs'=8,'tp'=2] {'rep','tp'}, use_global_device_ids=true, to_apply=%region_7.9 | all-reduce | flops 1280 | bytes 10240 | tf_op jit(solution)/shard_map/psum | solution.py:157
  389.7 30.0 %all-gather.17.cloned.1.call-done = bf16[2048,512]{1,0:T(8,128)(2,1)} async-done(((bf16[256,512]{1,0:T(8,128)(2,1)}), bf16[2048,512]{1,0:T(8,128)(2,1)}) %all-gather.17.cloned.1.call-update) | async-done | bytes 2097168 | tf_op jit(solution)/shard_map/all_gather | solution.py:120
  419.6 2.7 convolution_convert_fusion.5
  426.4 15.3 %collective-permute-done.9 = bf16[160,2048]{1,0:T(8,128)(2,1)S(1)} collective-permute-done((bf16[160,2048]{1,0:T(8,128)(2,1)S(1)}, bf16[160,2048]{1,0:T(8,128)(2,1)S(1)}, u32[]{:S(2)}, u32[]{:S(2)}) %collective-permute-start.9) | collective-permute-done | bytes 655392 | tf_op jit(solution)/shard_map/ppermute | solution.py:66
  444.1 14.5 %collective-permute-done.11 = bf16[160,2048]{1,0:T(8,128)(2,1)S(1)} collective-permute-done((bf16[160,2048]{1,0:T(8,128)(2,1)S(1)}, bf16[160,2048]{1,0:T(8,128)(2,1)S(1)}, u32[]{:S(2)}, u32[]{:S(2)}) %collective-permute-start.11) | collective-permute-done | bytes 655392 | tf_op jit(solution)/shard_map/ppermute | solution.py:61
  459.1 3.1 convolution_multiply_fusion.1
  462.3 3.1 convolution_multiply_fusion.3
  465.4 8.6 %convolution_convert_fusion.1 = bf16[320,2048]{1,0:T(8,128)(2,1)S(1)} fusion(bf16[2048,1280]{1,0:T(8,128)(2,1)} %all-gather.11.cloned.1.call-done, bf16[2048,1280]{1,0:T(8,128)(2,1)} %all-gather.9.cloned.1.call-done, f32[320,1280]{1,0:T(8,128)} %convolution_multiply_fusion.3, bf16[160,2048]{1,0:T(8,128)(2,1)S(1)} %get-tuple-element.23, ...), kind=kOutput, calls=%fused_computation.19 | convolution fusion | flops 3361587200 | bytes 14750720 | tf_op jit(solution)/shard_map/dot_general | solution.py:79
  474.6 10.1 %convolution_convert_fusion = bf16[320,2048]{1,0:T(8,128)(2,1)} fusion(bf16[2048,1280]{1,0:T(8,128)(2,1)} %all-gather.11.cloned.1.call-done, bf16[2048,1280]{1,0:T(8,128)(2,1)} %all-gather.9.cloned.1.call-done, f32[320,1280]{1,0:T(8,128)} %convolution_multiply_fusion.1, bf16[160,2048]{1,0:T(8,128)(2,1)} %copy-done.7, bf16[160,2048]{1,0:T(8,128)(2,1)} %copy-done.6, ...), kind=kOutput, calls=%fused_computation.18 | convolution fusion | flops 3361587200 | bytes 14750720 | tf_op jit(solution)/shard_map/dot_general | solution.py:79
  488.1 15.3 %collective-permute-done.14 = bf16[160,2048]{1,0:T(8,128)(2,1)S(1)} collective-permute-done((bf16[160,2048]{1,0:T(8,128)(2,1)S(1)}, bf16[160,2048]{1,0:T(8,128)(2,1)S(1)}, u32[]{:S(2)}, u32[]{:S(2)}) %collective-permute-start.14) | collective-permute-done | bytes 655392 | tf_op jit(solution)/shard_map/ppermute | solution.py:66
  504.0 2.1 collective-permute-done.17
  (146 shorter events, 32.7 us)
Async XLA Ops:
  6.5 91.6 %all-gather.7.cloned.1.call-start = ((), (), s32[]{:S(2)}) async-start(), calls=%async_computation | async-start | bytes 5898240 | tf_op jit(solution)/shard_map/all_gather | solution.py:120
  9.2 175.2 %all-gather.11.cloned.1.call-start = ((), (), s32[]{:S(2)}) async-start(), calls=%async_computation.2 | async-start | bytes 5898240 | tf_op jit(solution)/shard_map/all_gather | solution.py:120
  11.5 259.2 %all-gather.9.cloned.1.call-start = ((), (), s32[]{:S(2)}) async-start(), calls=%async_computation.1 | async-start | bytes 5898240 | tf_op jit(solution)/shard_map/all_gather | solution.py:120
  14.0 326.5 %all-gather.15.cloned.1.call-start = ((), (), s32[]{:S(2)}) async-start(), calls=%async_computation.4 | async-start | bytes 2359296 | tf_op jit(solution)/shard_map/all_gather | solution.py:120
  15.8 20.2 %copy-start.14 = (f32[2560]{0:T(1024)S(1)}, f32[2560]{0:T(1024)}, u32[]{:S(2)}) copy-start(f32[2560]{0:T(1024)} %param.27) | copy-start | bytes 30724
  15.8 20.3 %copy-start.15 = (f32[2560]{0:T(1024)S(1)}, f32[2560]{0:T(1024)}, u32[]{:S(2)}) copy-start(f32[2560]{0:T(1024)} %param.28) | copy-start | bytes 30724
  15.8 354.2 %all-gather.13.cloned.1.call-start = ((), (), s32[]{:S(2)}) async-start(), calls=%async_computation.3 | async-start | bytes 2359296 | tf_op jit(solution)/shard_map/all_gather | solution.py:120
  16.4 17.8 %collective-permute-start = (bf16[160,2048]{1,0:T(8,128)(2,1)S(1)}, bf16[160,2048]{1,0:T(8,128)(2,1)S(1)}, u32[]{:S(2)}, u32[]{:S(2)}) collective-permute-start(bf16[160,2048]{1,0:T(8,128)(2,1)S(1)} %fusion.13), channel_id=1, source_target_pairs={{0,16},{16,0},{1,17},{17,1},{2,18},{18,2},{3,19},{19,3},{4,20},{20... | collective-permute-start | bytes 1966088 | tf_op jit(solution)/shard_map/ppermute | solution.py:61
  34.1 2.4 collective-permute-start.1
  35.9 383.7 %all-gather.17.cloned.1.call-start = ((), (), s32[]{:S(2)}) async-start(), calls=%async_computation.5 | async-start | bytes 2359296 | tf_op jit(solution)/shard_map/all_gather | solution.py:120
  37.5 66.5 %copy-start.8 = (bf16[160,2048]{1,0:T(8,128)(2,1)}, bf16[160,2048]{1,0:T(8,128)(2,1)S(1)}, u32[]{:S(2)}) copy-start(bf16[160,2048]{1,0:T(8,128)(2,1)S(1)} %get-tuple-element.30) | copy-start | bytes 1966084
  98.2 172.6 %copy-start.9 = (bf16[160,2048]{1,0:T(8,128)(2,1)S(1)}, bf16[160,2048]{1,0:T(8,128)(2,1)}, u32[]{:S(2)}) copy-start(bf16[160,2048]{1,0:T(8,128)(2,1)} %get-tuple-element.31) | copy-start | bytes 1966084
  280.6 14.9 %collective-permute-start.2 = (bf16[160,2048]{1,0:T(8,128)(2,1)}, bf16[160,2048]{1,0:T(8,128)(2,1)S(1)}, u32[]{:S(2)}, u32[]{:S(2)}) collective-permute-start(bf16[160,2048]{1,0:T(8,128)(2,1)} %constant_dynamic-slice_fusion.6), channel_id=1, source_target_pairs={{0,1},{1,0},{2,3},{3,2},{4,5},{5,4},{6,7},{7,6},{8,9},{9,8},{10,11... | collective-permute-start | bytes 1966088 | tf_op jit(solution)/shard_map/ppermute | solution.py:37
  295.2 29.7 %collective-permute-start.4 = (bf16[160,2048]{1,0:T(8,128)(2,1)S(1)}, bf16[160,2048]{1,0:T(8,128)(2,1)S(1)}, u32[]{:S(2)}, u32[]{:S(2)}) collective-permute-start(bf16[160,2048]{1,0:T(8,128)(2,1)S(1)} %constant_dynamic-slice_fusion.5), channel_id=1, source_target_pairs={{0,1},{1,0},{2,3},{3,2},{4,5},{5,4},{6,7},{7,6},{8,9},{9,8},{10,11... | collective-permute-start | bytes 1966088 | tf_op jit(solution)/shard_map/ppermute | solution.py:37
  296.6 28.3 %collective-permute-start.3 = (bf16[160,2048]{1,0:T(8,128)(2,1)S(1)}, bf16[160,2048]{1,0:T(8,128)(2,1)S(1)}, u32[]{:S(2)}, u32[]{:S(2)}) collective-permute-start(bf16[160,2048]{1,0:T(8,128)(2,1)S(1)} %add_convert_fusion.2), channel_id=1, source_target_pairs={{0,16},{16,0},{1,17},{17,1},{2,18},{18,2},{3,19},{19,3},{4,20},{20... | collective-permute-start | bytes 1966088 | tf_op jit(solution)/shard_map/ppermute | solution.py:66
  325.9 13.3 %collective-permute-start.5 = (bf16[160,2048]{1,0:T(8,128)(2,1)S(1)}, bf16[160,2048]{1,0:T(8,128)(2,1)S(1)}, u32[]{:S(2)}, u32[]{:S(2)}) collective-permute-start(bf16[160,2048]{1,0:T(8,128)(2,1)S(1)} %fusion.17), channel_id=1, source_target_pairs={{0,16},{16,0},{1,17},{17,1},{2,18},{18,2},{3,19},{19,3},{4,20},{20... | collective-permute-start | bytes 1966088 | tf_op jit(solution)/shard_map/ppermute | solution.py:61
  326.5 12.7 %collective-permute-start.7 = (bf16[160,2048]{1,0:T(8,128)(2,1)S(1)}, bf16[160,2048]{1,0:T(8,128)(2,1)S(1)}, u32[]{:S(2)}, u32[]{:S(2)}) collective-permute-start(bf16[160,2048]{1,0:T(8,128)(2,1)S(1)} %fusion.17), channel_id=1, source_target_pairs={{0,1},{1,0},{2,3},{3,2},{4,5},{5,4},{6,7},{7,6},{8,9},{9,8},{10,11... | collective-permute-start | bytes 1966088 | tf_op jit(solution)/shard_map/ppermute | solution.py:37
  339.2 36.6 %collective-permute-start.6 = (bf16[160,2048]{1,0:T(8,128)(2,1)S(1)}, bf16[160,2048]{1,0:T(8,128)(2,1)S(1)}, u32[]{:S(2)}, u32[]{:S(2)}) collective-permute-start(bf16[160,2048]{1,0:T(8,128)(2,1)S(1)} %collective-permute-done.5), channel_id=1, source_target_pairs={{0,1},{1,0},{2,3},{3,2},{4,5},{5,4},{6,7},{7,6},{8,9},{9,8},{10,11... | collective-permute-start | bytes 1966088 | tf_op jit(solution)/shard_map/ppermute | solution.py:37
  340.5 29.5 %copy-start.10 = (bf16[160,2048]{1,0:T(8,128)(2,1)S(1)}, bf16[160,2048]{1,0:T(8,128)(2,1)}, u32[]{:S(2)}) copy-start(bf16[160,2048]{1,0:T(8,128)(2,1)} %get-tuple-element.29) | copy-start | bytes 1966084
  419.6 39.4 %slice-start = ((s8[5242880]{0:T(1024)(128)(4,1)}), s8[4194304]{0:T(1024)(128)(4,1)S(1)}, s32[]{:S(2)}) async-start(s8[5242880]{0:T(1024)(128)(4,1)} %bitcast.124), calls=%async_computation.6 | async-start | bytes 8388608
  422.4 2.2 collective-permute-start.8
  422.5 36.5 %slice-start.1 = ((s8[5242880]{0:T(1024)(128)(4,1)}), s8[1048576]{0:T(1024)(128)(4,1)S(1)}, s32[]{:S(2)}) async-start(s8[5242880]{0:T(1024)(128)(4,1)} %bitcast.124), calls=%async_computation.7 | async-start | bytes 2097152
  423.6 2.8 collective-permute-start.10
  424.8 16.8 %collective-permute-start.9 = (bf16[160,2048]{1,0:T(8,128)(2,1)S(1)}, bf16[160,2048]{1,0:T(8,128)(2,1)S(1)}, u32[]{:S(2)}, u32[]{:S(2)}) collective-permute-start(bf16[160,2048]{1,0:T(8,128)(2,1)S(1)} %add_convert_fusion.1), channel_id=1, source_target_pairs={{0,16},{16,0},{1,17},{17,1},{2,18},{18,2},{3,19},{19,3},{4,20},{20... | collective-permute-start | bytes 1966088 | tf_op jit(solution)/shard_map/ppermute | solution.py:66
  442.6 16.0 %collective-permute-start.11 = (bf16[160,2048]{1,0:T(8,128)(2,1)S(1)}, bf16[160,2048]{1,0:T(8,128)(2,1)S(1)}, u32[]{:S(2)}, u32[]{:S(2)}) collective-permute-start(bf16[160,2048]{1,0:T(8,128)(2,1)S(1)} %fusion.21), channel_id=1, source_target_pairs={{0,16},{16,0},{1,17},{17,1},{2,18},{18,2},{3,19},{19,3},{4,20},{20... | collective-permute-start | bytes 1966088 | tf_op jit(solution)/shard_map/ppermute | solution.py:61
  444.1 14.5 %collective-permute-start.15 = (bf16[160,2048]{1,0:T(8,128)(2,1)S(1)}, bf16[160,2048]{1,0:T(8,128)(2,1)S(1)}, u32[]{:S(2)}, u32[]{:S(2)}) collective-permute-start(bf16[160,2048]{1,0:T(8,128)(2,1)S(1)} %fusion.21), channel_id=1, source_target_pairs={{0,1},{1,0},{2,3},{3,2},{4,5},{5,4},{6,7},{7,6},{8,9},{9,8},{10,11... | collective-permute-start | bytes 1966088 | tf_op jit(solution)/shard_map/ppermute | solution.py:37
  458.6 3.6 collective-permute-start.12
  474.1 12.0 %collective-permute-start.13 = (bf16[160,2048]{1,0:T(8,128)(2,1)S(1)}, bf16[160,2048]{1,0:T(8,128)(2,1)S(1)}, u32[]{:S(2)}, u32[]{:S(2)}) collective-permute-start(bf16[160,2048]{1,0:T(8,128)(2,1)S(1)} %constant_dynamic-slice_fusion.2), channel_id=1, source_target_pairs={{0,1},{1,0},{2,3},{3,2},{4,5},{5,4},{6,7},{7,6},{8,9},{9,8},{10,11... | collective-permute-start | bytes 1966088 | tf_op jit(solution)/shard_map/ppermute | solution.py:37
  484.7 18.7 %copy-start.5 = (bf16[320,2048]{1,0:T(8,128)(2,1)S(1)}, bf16[320,2048]{1,0:T(8,128)(2,1)}, u32[]{:S(2)}) copy-start(bf16[320,2048]{1,0:T(8,128)(2,1)} %convolution_convert_fusion) | copy-start | bytes 3932164
  485.9 2.2 collective-permute-start.16
  486.2 17.2 %collective-permute-start.14 = (bf16[160,2048]{1,0:T(8,128)(2,1)S(1)}, bf16[160,2048]{1,0:T(8,128)(2,1)S(1)}, u32[]{:S(2)}, u32[]{:S(2)}) collective-permute-start(bf16[160,2048]{1,0:T(8,128)(2,1)S(1)} %add_convert_fusion), channel_id=1, source_target_pairs={{0,16},{16,0},{1,17},{17,1},{2,18},{18,2},{3,19},{19,3},{4,20},{20... | collective-permute-start | bytes 1966088 | tf_op jit(solution)/shard_map/ppermute | solution.py:66
  503.9 2.2 collective-permute-start.17
  (18 other events, 44.0 us)
Sparse Core Ops, SparseCore 0:
  9.5 88.5 all-gather.6
  100.3 84.0 all-gather.10
  186.6 84.0 all-gather.8
  272.7 47.4 all-gather.14
  322.2 47.7 all-gather.12
  372.0 47.6 all-gather.16
